TPU v7x, 128 devices: a whole 4x4x4 slice. The times are simulated.
128 devices in a mesh: ra: 16 (over z, x), cb: 4 (over y), dp: 2 (over core).
Axes of the slice: x: 4, y: 4, z: 4, core: 2. Of those that a mesh axis runs over, the one named last changes fastest.
Arguments:
- carried: bfloat16 [3072, 4096], P('dp', 'ra'), may hold values from -100 to 100
- branch_in: bfloat16 [3072, 4096], P('dp', 'ra'), may hold values from -12 to 12
- gain_in: float32 [4096], P('ra'), may hold values from 0.1 to 1.9
- bias_in: float32 [4096], P('ra'), may hold values from -1.8 to 1.8
- up_weight: bfloat16 [4096, 16384], P('ra', 'cb'), may hold values from -0.125 to 0.125
- down_weight: bfloat16 [16384, 4096], P('cb', 'ra'), may hold values from -0.046875 to 0.046875
- gain_out: float32 [4096], P('ra'), may hold values from 0.1 to 1.9
- bias_out: float32 [4096], P('ra'), may hold values from -1.8 to 1.8
Outputs:
- layer_out: bfloat16 [3072, 4096], P('dp', 'ra')
All inputs are finite; a program needn't handle non-finite values.
Results may differ from a plain program's by a relative error of at most 0.006.
Values may be sent and summed in bfloat16 or wider, within the bound.
A program may use at most 64 MiB of HBM per device.

v0:
```python
import jax
import jax.numpy as jnp
from jax import lax
from jax.sharding import PartitionSpec as P

residual_scale = 2.0**0.25
norm_eps = 1e-05


def copy_for_each(array, axis):
    length = lax.axis_size(axis)
    return lax.all_to_all(
        jnp.broadcast_to(array[None], (length, *array.shape)), axis, 0, 0, tiled=True
    )


def of_everyone(array, axis):
    return copy_for_each(array, axis).sum(axis=0)


def packed_total(arrays, axis):
    ravelled, at, done = (jnp.concatenate([a.reshape(-1) for a in arrays]), 0, [])
    running = of_everyone(ravelled, axis)
    for a in arrays:
        done.append(running[at : at + a.size].reshape(a.shape))
        at += a.size
    return tuple(done)


def taken_together(array, axis):
    return copy_for_each(array, axis).astype(jnp.float32).sum(axis=0)


def normalize(mixed, totals, squares, width, gain, bias):
    mean = totals[:, None] / width
    spread = squares[:, None] / width - mean * mean
    return (mixed - mean) * lax.rsqrt(spread + norm_eps) * gain + bias


def per_device(carried, branch_in, gain_in, bias_in, up_weight, down_weight, gain_out, bias_out):
    width = carried.shape[1] * lax.axis_size("ra")
    mixed_in = residual_scale * carried.astype(jnp.float32) + branch_in.astype(jnp.float32)
    totals, squares = packed_total(
        (jnp.sum(mixed_in, axis=1), jnp.sum(mixed_in * mixed_in, axis=1)), "ra"
    )
    normed = normalize(mixed_in, totals, squares, width, gain_in, bias_in).astype(jnp.bfloat16)
    regrouped = lax.all_to_all(up_weight, "ra", split_axis=1, concat_axis=0, tiled=True)
    pre_share = lax.dot_general(
        regrouped,
        lax.all_gather(normed, "ra", axis=1, tiled=True),
        (((0,), (1,)), ((), ())),
        preferred_element_type=jnp.float32,
    )
    hidden_share = jnp.square(jnp.maximum(pre_share, 0.0)).astype(jnp.bfloat16)
    branch_part = lax.dot_general(
        lax.all_gather(hidden_share, "ra", axis=0, tiled=True),
        down_weight,
        (((0,), (0,)), ((), ())),
        preferred_element_type=jnp.float32,
    )
    branch_out = taken_together(branch_part.astype(jnp.bfloat16), "cb").astype(jnp.float32)
    mixed_out = residual_scale * normed.astype(jnp.float32) + branch_out
    totals_out, squares_out = packed_total(
        (jnp.sum(mixed_out, axis=1), jnp.sum(mixed_out * mixed_out, axis=1)), "ra"
    )
    return normalize(mixed_out, totals_out, squares_out, width, gain_out, bias_out).astype(
        jnp.bfloat16
    )


def solution(mesh):
    in_specs = (
        P("dp", "ra"),
        P("dp", "ra"),
        P("ra"),
        P("ra"),
        P("ra", "cb"),
        P("cb", "ra"),
        P("ra"),
        P("ra"),
    )
    out_specs = P("dp", "ra")
    return jax.shard_map(
        per_device, mesh=mesh, in_specs=in_specs, out_specs=out_specs, check_vma=False
    )
```

profile of v0, /device:TPU:0, one launch (start us, length us, event | category | flops | bytes accessed | tf_op | source)
XLA Modules:
  0.0 324.9 jit_solution(11136814874928397678)
XLA Ops:
  6.5 0.0 copy-start
  6.5 0.0 copy-start.3
  6.5 0.0 copy-start.4
  6.5 0.0 copy-start.5
  6.5 0.0 all-gather.3.cloned.1.call-start
  6.6 2.1 fusion.3
  8.7 0.1 broadcast_in_dim.6
  8.8 16.1 %all_to_all.36 = f32[16,1,3072]{2,1,0:T(1,128)S(1)} all-to-all(f32[16,1,3072]{2,1,0:T(1,128)S(1)} %broadcast_in_dim.6), channel_id=1, replica_groups=mesh['ra'=16,'cb'=4,'dp'=2] {'ra'}, dimensions={0} | all-to-all | bytes 393216 | tf_op jit(solution)/shard_map/all_to_all | solution.py:12
  24.9 0.1 reduce_sum.65
  25.1 0.0 copy-done.3
  25.1 0.0 copy-done.4
  25.1 0.0 copy-done.5
  25.1 2.5 add_convert_fusion.1
  27.6 0.0 all-gather.3.cloned.1.call-update
  27.6 0.0 all-gather.5.cloned.1.call-start
  27.7 4.1 %copy.14 = bf16[256,4096]{0,1:T(8,128)(2,1)} copy(bf16[256,4096]{1,0:T(8,128)(2,1)} %param.12) | data formatting | bytes 4194304 | tf_op args[4]
  31.7 44.3 %all_to_all.37 = bf16[256,16,256]{0,2,1:T(8,128)(2,1)} all-to-all(bf16[256,16,256]{0,2,1:T(8,128)(2,1)} %bitcast.10), channel_id=1, replica_groups=mesh['ra'=16,'cb'=4,'dp'=2] {'ra'}, dimensions={1} | all-to-all | bytes 4194304 | tf_op jit(solution)/shard_map/all_to_all | solution.py:47
  76.0 3.9 %copy.15 = bf16[16,256,256]{2,1,0:T(8,128)(2,1)} copy(bf16[16,256,256]{1,2,0:T(8,128)(2,1)} %bitcast.9) | data formatting | bytes 4194304 | tf_op jit(solution)/shard_map/all_to_all | solution.py:47
  79.9 65.2 %all-gather.3.cloned.1.call-done = bf16[1536,4096]{1,0:T(8,128)(2,1)} async-done(((bf16[1536,256]{1,0:T(8,128)(2,1)}), bf16[1536,4096]{1,0:T(8,128)(2,1)}) %all-gather.3.cloned.1.call-update) | async-done | bytes 12582928 | tf_op jit(solution)/shard_map/all_gather | solution.py:50
  145.1 9.6 %fusion.2 = bf16[256,1536]{0,1:T(8,128)(2,1)} fusion(bf16[1536,4096]{1,0:T(8,128)(2,1)} %all-gather.3.cloned.1.call-done, bf16[4096,256]{1,0:T(8,128)(2,1)} %bitcast.11), kind=kOutput, calls=%fused_computation.5 | convolution fusion | flops 3222405120 | bytes 15466496 | tf_op jit(solution)/shard_map/dot_general | solution.py:48
  154.7 0.0 all-gather.5.cloned.1.call-update
  154.7 98.0 %all-gather.5.cloned.1.call-done = bf16[4096,1536]{0,1:T(8,128)(2,1)} async-done(((bf16[256,1536]{0,1:T(8,128)(2,1)}), bf16[4096,1536]{0,1:T(8,128)(2,1)}) %all-gather.5.cloned.1.call-update) | async-done | bytes 12582928 | tf_op jit(solution)/shard_map/all_gather | solution.py:56
  252.8 0.0 copy-done
  252.8 6.5 %convolution_convert_fusion = bf16[1536,256]{1,0:T(8,128)(2,1)S(1)} fusion(bf16[4096,1536]{0,1:T(8,128)(2,1)} %all-gather.5.cloned.1.call-done, bf16[4096,256]{1,0:T(8,128)(2,1)S(1)} %copy-done), kind=kOutput, calls=%fused_computation.4 | convolution fusion | flops 3221618688 | bytes 15466496 | tf_op jit(solution)/shard_map/dot_general | solution.py:55
  259.3 0.2 broadcast_in_dim.7
  259.5 40.3 %all_to_all.38 = bf16[4,1536,256]{2,1,0:T(8,128)(2,1)S(1)} all-to-all(bf16[4,1536,256]{2,1,0:T(8,128)(2,1)S(1)} %broadcast_in_dim.7), channel_id=1, replica_groups=mesh['ra'=16,'cb'=4,'dp'=2] {'cb'}, dimensions={0} | all-to-all | bytes 6291456 | tf_op jit(solution)/shard_map/all_to_all | solution.py:12
  299.8 0.0 copy-start.2
  299.8 0.5 convert_reduce_fusion
  300.2 0.0 copy-start.1
  300.2 1.1 copy-done.1
  301.4 0.0 copy-done.2
  301.4 0.0 copy-start.6
  301.4 0.0 copy-start.7
  301.4 0.5 fusion.4
  301.9 0.1 broadcast_in_dim.8
  302.0 13.1 %all_to_all.39 = f32[16,1,3072]{2,1,0:T(1,128)S(1)} all-to-all(f32[16,1,3072]{2,1,0:T(1,128)S(1)} %broadcast_in_dim.8), channel_id=1, replica_groups=mesh['ra'=16,'cb'=4,'dp'=2] {'ra'}, dimensions={0} | all-to-all | bytes 393216 | tf_op jit(solution)/shard_map/all_to_all | solution.py:12
  315.1 0.1 reduce_sum.69
  315.3 0.0 copy-done.6
  315.3 0.0 copy-done.7
  315.3 2.8 add_convert_fusion
  (4 shorter events, 0.0 us)
Async XLA Ops:
  6.5 246.2 %copy-start = (bf16[4096,256]{1,0:T(8,128)(2,1)S(1)}, bf16[4096,256]{1,0:T(8,128)(2,1)}, u32[]{:S(2)}) copy-start(bf16[4096,256]{1,0:T(8,128)(2,1)} %param.13) | copy-start | bytes 6291460
  6.5 18.5 %copy-start.3 = (bf16[1536,256]{1,0:T(8,128)(2,1)S(1)}, bf16[1536,256]{1,0:T(8,128)(2,1)}, u32[]{:S(2)}) copy-start(bf16[1536,256]{1,0:T(8,128)(2,1)} %param.9) | copy-start | bytes 2359300
  6.5 18.5 %copy-start.4 = (f32[256]{0:T(256)S(1)}, f32[256]{0:T(256)}, u32[]{:S(2)}) copy-start(f32[256]{0:T(256)} %param.11) | copy-start | bytes 3076
  6.5 18.5 %copy-start.5 = (f32[256]{0:T(256)S(1)}, f32[256]{0:T(256)}, u32[]{:S(2)}) copy-start(f32[256]{0:T(256)} %param.10) | copy-start | bytes 3076
  6.5 138.6 %all-gather.3.cloned.1.call-start = ((), (), s32[]{:S(2)}) async-start(), calls=%async_computation.4 | async-start | bytes 13369344 | tf_op jit(solution)/shard_map/all_gather | solution.py:50
  27.6 225.1 %all-gather.5.cloned.1.call-start = ((), (), s32[]{:S(2)}) async-start(), calls=%async_computation.5 | async-start | bytes 13369344 | tf_op jit(solution)/shard_map/all_gather | solution.py:56
  299.8 1.6 copy-start.2
  300.2 1.2 copy-start.1
  301.4 13.9 %copy-start.6 = (f32[256]{0:T(256)S(1)}, f32[256]{0:T(256)}, u32[]{:S(2)}) copy-start(f32[256]{0:T(256)} %param.15) | copy-start | bytes 3076
  301.4 13.9 %copy-start.7 = (f32[256]{0:T(256)S(1)}, f32[256]{0:T(256)}, u32[]{:S(2)}) copy-start(f32[256]{0:T(256)} %param.14) | copy-start | bytes 3076
Sparse Core Ops, SparseCore 0:
  27.7 117.3 all-gather.2
  154.9 97.8 all-gather.4
where the time goes:
time: 325 us
  waiting for transfers between devices  163 us (50%)
  blocking collectives  114 us (35%)
  matrix products  16.1 us (5%)
  between operations  13.5 us (4%)
  local copies, waits for them, and re-layouts  9.57 us (3%)
  other arithmetic  8.59 us (3%)
    all_gather x1, waiting for transfers between devices, per_device(): lax.all_gather(hidden_share, 'ra', axis=0, tiled=True)  98 us
    all_to_all x3, blocking collectives, copy_for_each(): lax.all_to_all(jnp.broadcast_to(array[None], (length, *array.shape)), axi...  69.5 us
    all_gather x1, waiting for transfers between devices, per_device(): lax.all_gather(normed, 'ra', axis=1, tiled=True)  65.2 us
    all_to_all x1, blocking collectives, per_device(): lax.all_to_all(up_weight, 'ra', split_axis=1, concat_axis=0, tiled=True)  44.3 us
    dot_general x1, matrix products, per_device(): lax.dot_general(regrouped, lax.all_gather(normed, 'ra', axis=1, tiled=Tru...  9.57 us
  transfers between devices with their start and end apart: 2, of which 2 were waited for; matrix products, arithmetic and copies ran while one was open for 2% of the time, Pallas kernels for 0%

commit v1 on v0

--- a/solution.py
+++ b/solution.py
@@ -5,6 +5,21 @@
 
 residual_scale = 2.0**0.25
 norm_eps = 1e-05
+
+
+def supply_all_links(array_in):
+    all_rows, all_values = (lax.psum(1, "ra"), lax.axis_index("ra"))
+    local_now, u_next = (array_in, 1)
+    while u_next < all_rows:
+        line_up = []
+        for k0 in tuple(range(all_rows)):
+            line_up.append((k0, k0 ^ u_next))
+        mat_out = lax.ppermute(local_now, "ra", perm=line_up)
+        mid_arr = jnp.concatenate([local_now, mat_out], 1)
+        b_now = jnp.concatenate([mat_out, local_now], 1)
+        local_now = jnp.where(all_values & u_next == 0, mid_arr, b_now)
+        u_next = 2 * u_next
+    return local_now
 
 
 def copy_for_each(array, axis):
@@ -47,7 +62,7 @@
     regrouped = lax.all_to_all(up_weight, "ra", split_axis=1, concat_axis=0, tiled=True)
     pre_share = lax.dot_general(
         regrouped,
-        lax.all_gather(normed, "ra", axis=1, tiled=True),
+        supply_all_links(normed),
         (((0,), (1,)), ((), ())),
         preferred_element_type=jnp.float32,
     )

time: 325 us -> 510 us (1.57)
  waiting for transfers between devices: 163 us -> 363 us
  blocking collectives: 114 us -> 69.5 us
  other arithmetic: 8.59 us -> 26.3 us
  starting transfers between devices: 0.08 us -> 8.53 us
    all_to_all x0 -> x1, waiting for transfers between devices: none -> 147 us  [per_device(): lax.all_to_all(up_weight, 'ra', split_axis=1, concat_axis=0, tiled=True)]
    ppermute x0 -> x4, waiting for transfers between devices: none -> 119 us  [supply_all_links(): mat_out = lax.ppermute(local_now, 'ra', perm=line_up)]
    all_gather x1 -> x0, waiting for transfers between devices: 65.2 us -> none  [per_device(): lax.all_gather(normed, 'ra', axis=1, tiled=True)]
    all_to_all x1 -> x0, blocking collectives: 44.3 us -> none  [per_device(): lax.all_to_all(up_weight, 'ra', split_axis=1, concat_axis=0, tiled=True)]
    select_n x0 -> x3, other arithmetic: none -> 18.4 us  [supply_all_links(): local_now = jnp.where(all_values & u_next == 0, mid_arr, b_now)]
  transfers between devices with their start and end apart: 2 -> 6, of which waited for: 2 -> 5; matrix products, arithmetic and copies ran while one was open for 2% -> 2% of each run, Pallas kernels for 0% -> 0%
where the time goes in v1:
time: 510 us
  waiting for transfers between devices  363 us (71%)
  blocking collectives  69.5 us (14%)
  other arithmetic  26.3 us (5%)
  matrix products  19 us (4%)
  between operations  13.6 us (3%)
  local copies, waits for them, and re-layouts  9.55 us (2%)
  starting transfers between devices  8.53 us (2%)
    all_to_all x1, waiting for transfers between devices, per_device(): lax.all_to_all(up_weight, 'ra', split_axis=1, concat_axis=0, tiled=True)  147 us
    ppermute x4, waiting for transfers between devices, supply_all_links(): mat_out = lax.ppermute(local_now, 'ra', perm=line_up)  119 us
    all_gather x1, waiting for transfers between devices, per_device(): lax.all_gather(hidden_share, 'ra', axis=0, tiled=True)  97.6 us
    all_to_all x3, blocking collectives, copy_for_each(): lax.all_to_all(jnp.broadcast_to(array[None], (length, *array.shape)), axi...  69.5 us
    select_n x3, other arithmetic, supply_all_links(): local_now = jnp.where(all_values & u_next == 0, mid_arr, b_now)  18.4 us
    dot_general x1, matrix products, per_device(): lax.dot_general(regrouped, supply_all_links(normed), (((0,), (1,)), ((),...  12.5 us
  transfers between devices with their start and end apart: 6, of which 5 were waited for; matrix products, arithmetic and copies ran while one was open for 2% of the time, Pallas kernels for 0%

profile of v1, /device:TPU:0, one launch (start us, length us, event | category | flops | bytes accessed | tf_op | source)
XLA Modules:
  0.0 510.0 jit_solution(7866510448810644576)
XLA Ops:
  6.5 0.0 copy-start
  6.5 0.0 copy-start.2
  6.5 0.0 copy-start.3
  6.5 2.1 fusion.11
  8.6 0.1 broadcast_in_dim.6
  8.7 16.1 %all_to_all.36 = f32[16,1,3072]{2,1,0:T(1,128)S(1)} all-to-all(f32[16,1,3072]{2,1,0:T(1,128)S(1)} %broadcast_in_dim.6), channel_id=1, replica_groups=mesh['ra'=16,'cb'=4,'dp'=2] {'ra'}, dimensions={0} | all-to-all | bytes 393216 | tf_op jit(solution)/shard_map/all_to_all | solution.py:27
  24.9 0.1 reduce_sum.65
  25.0 0.0 copy-done.2
  25.0 0.0 copy-done.3
  25.0 1.8 add_convert_fusion.1
  26.9 0.6 collective-permute-start
  27.5 17.4 %collective-permute-done = bf16[1536,256]{1,0:T(8,128)(2,1)} collective-permute-done((bf16[1536,256]{1,0:T(8,128)(2,1)S(1)}, bf16[1536,256]{1,0:T(8,128)(2,1)}, u32[]{:S(2)}, u32[]{:S(2)}) %collective-permute-start) | collective-permute-done | bytes 786464 | tf_op jit(solution)/shard_map/ppermute | solution.py:17
  44.9 2.9 maximum_select_fusion.12
  47.8 1.4 collective-permute-start.1
  49.2 34.3 %collective-permute-done.1 = bf16[1536,512]{1,0:T(8,128)(2,1)} collective-permute-done((bf16[1536,512]{1,0:T(8,128)(2,1)}, bf16[1536,512]{1,0:T(8,128)(2,1)}, u32[]{:S(2)}, u32[]{:S(2)}) %collective-permute-start.1) | collective-permute-done | bytes 1572896 | tf_op jit(solution)/shard_map/ppermute | solution.py:17
  83.5 5.3 %maximum_select_fusion.3 = bf16[1536,1024]{1,0:T(8,128)(2,1)} fusion(bf16[1536,512]{1,0:T(8,128)(2,1)} %collective-permute-done.1, bf16[1536,512]{1,0:T(8,128)(2,1)} %maximum_select_fusion.12, pred[]{:T(512)S(6)} %eq.14), kind=kLoop, calls=%fused_computation.10 | loop fusion | flops 14155776 | bytes 6291457 | tf_op jit(solution)/shard_map/jit(_where)/select_n | solution.py:20
  88.8 0.1 collective-permute-start.2
  88.9 66.9 %collective-permute-done.2 = bf16[1536,1024]{1,0:T(8,128)(2,1)} collective-permute-done((bf16[1536,1024]{1,0:T(8,128)(2,1)}, bf16[1536,1024]{1,0:T(8,128)(2,1)}, u32[]{:S(2)}, u32[]{:S(2)}) %collective-permute-start.2) | collective-permute-done | bytes 3145760 | tf_op jit(solution)/shard_map/ppermute | solution.py:17
  155.8 10.2 %maximum_select_fusion.2 = bf16[1536,2048]{1,0:T(8,128)(2,1)} fusion(bf16[1536,1024]{1,0:T(8,128)(2,1)} %collective-permute-done.2, bf16[1536,1024]{1,0:T(8,128)(2,1)} %maximum_select_fusion.3, pred[]{:T(512)S(6)} %eq.13), kind=kLoop, calls=%fused_computation.8 | loop fusion | flops 28311552 | bytes 12582913 | tf_op jit(solution)/shard_map/jit(_where)/select_n | solution.py:20
  166.0 1.8 collective-permute-start.3
  167.8 4.1 copy.14
  171.9 4.6 all-to-all-start.1
  176.4 0.0 all-gather.2.cloned.1.call-start
  176.5 147.3 %all-to-all-done.1 = bf16[256,16,256]{0,2,1:T(8,128)(2,1)} async-done(((bf16[256,16,256]{0,2,1:T(8,128)(2,1)}), bf16[256,16,256]{0,2,1:T(8,128)(2,1)}, u32[]{:S(2)}, u32[]{:S(2)}) %all-to-all-start.1) | async-done | bytes 2097184 | tf_op jit(solution)/shard_map/all_to_all | solution.py:62
  323.8 3.9 copy.15
  327.7 0.0 collective-permute-done.3
  327.7 12.5 %fusion.10 = bf16[256,1536]{0,1:T(8,128)(2,1)} fusion(bf16[4096,256]{1,0:T(8,128)(2,1)} %bitcast.9, bf16[1536,2048]{1,0:T(8,128)(2,1)} %collective-permute-done.3, bf16[1536,2048]{1,0:T(8,128)(2,1)} %maximum_select_fusion.2, pred[]{:T(512)S(6)} %eq.12), kind=kOutput, calls=%fused_computation.15 | convolution fusion | flops 3279028224 | bytes 15466497 | tf_op jit(solution)/shard_map/dot_general | solution.py:63
  340.2 0.0 all-gather.2.cloned.1.call-update
  340.3 97.6 %all-gather.2.cloned.1.call-done = bf16[4096,1536]{0,1:T(8,128)(2,1)} async-done(((bf16[256,1536]{0,1:T(8,128)(2,1)}), bf16[4096,1536]{0,1:T(8,128)(2,1)}) %all-gather.2.cloned.1.call-update) | async-done | bytes 12582928 | tf_op jit(solution)/shard_map/all_gather | solution.py:71
  437.8 0.0 copy-done
  437.8 6.5 %convolution_convert_fusion = bf16[1536,256]{1,0:T(8,128)(2,1)S(1)} fusion(bf16[4096,1536]{0,1:T(8,128)(2,1)} %all-gather.2.cloned.1.call-done, bf16[4096,256]{1,0:T(8,128)(2,1)S(1)} %copy-done), kind=kOutput, calls=%fused_computation.14 | convolution fusion | flops 3221618688 | bytes 15466496 | tf_op jit(solution)/shard_map/dot_general | solution.py:70
  444.3 0.2 broadcast_in_dim.7
  444.6 40.3 %all_to_all.37 = bf16[4,1536,256]{2,1,0:T(8,128)(2,1)S(1)} all-to-all(bf16[4,1536,256]{2,1,0:T(8,128)(2,1)S(1)} %broadcast_in_dim.7), channel_id=1, replica_groups=mesh['ra'=16,'cb'=4,'dp'=2] {'cb'}, dimensions={0} | all-to-all | bytes 6291456 | tf_op jit(solution)/shard_map/all_to_all | solution.py:27
  484.8 0.5 convert_reduce_fusion
  485.3 0.0 copy-start.1
  485.3 1.1 copy-done.1
  486.5 0.0 copy-start.4
  486.5 0.0 copy-start.5
  486.5 0.5 fusion.12
  487.0 0.1 broadcast_in_dim.8
  487.1 13.1 %all_to_all.38 = f32[16,1,3072]{2,1,0:T(1,128)S(1)} all-to-all(f32[16,1,3072]{2,1,0:T(1,128)S(1)} %broadcast_in_dim.8), channel_id=1, replica_groups=mesh['ra'=16,'cb'=4,'dp'=2] {'ra'}, dimensions={0} | all-to-all | bytes 393216 | tf_op jit(solution)/shard_map/all_to_all | solution.py:27
  500.2 0.1 reduce_sum.69
  500.4 0.0 copy-done.4
  500.4 0.0 copy-done.5
  500.4 2.8 add_convert_fusion
  (4 shorter events, 0.0 us)
Async XLA Ops:
  6.5 431.3 %copy-start = (bf16[4096,256]{1,0:T(8,128)(2,1)S(1)}, bf16[4096,256]{1,0:T(8,128)(2,1)}, u32[]{:S(2)}) copy-start(bf16[4096,256]{1,0:T(8,128)(2,1)} %param.13) | copy-start | bytes 6291460
  6.5 18.5 %copy-start.2 = (f32[256]{0:T(256)S(1)}, f32[256]{0:T(256)}, u32[]{:S(2)}) copy-start(f32[256]{0:T(256)} %param.11) | copy-start | bytes 3076
  6.5 18.5 %copy-start.3 = (f32[256]{0:T(256)S(1)}, f32[256]{0:T(256)}, u32[]{:S(2)}) copy-start(f32[256]{0:T(256)} %param.10) | copy-start | bytes 3076
  26.9 18.0 %collective-permute-start = (bf16[1536,256]{1,0:T(8,128)(2,1)S(1)}, bf16[1536,256]{1,0:T(8,128)(2,1)}, u32[]{:S(2)}, u32[]{:S(2)}) collective-permute-start(bf16[1536,256]{1,0:T(8,128)(2,1)S(1)} %add_convert_fusion.1), channel_id=1, source_target_pairs={{0,8},{8,0},{16,24},{24,16},{32,40},{40,32},{48,56},{56,48},{64,72... | collective-permute-start | bytes 2359304 | tf_op jit(solution)/shard_map/ppermute | solution.py:17
  47.8 35.7 %collective-permute-start.1 = (bf16[1536,512]{1,0:T(8,128)(2,1)}, bf16[1536,512]{1,0:T(8,128)(2,1)}, u32[]{:S(2)}, u32[]{:S(2)}) collective-permute-start(bf16[1536,512]{1,0:T(8,128)(2,1)} %maximum_select_fusion.12), channel_id=1, source_target_pairs={{0,16},{8,24},{16,0},{24,8},{32,48},{40,56},{48,32},{56,40},{64,80... | collective-permute-start | bytes 4718600 | tf_op jit(solution)/shard_map/ppermute | solution.py:17
  88.8 67.0 %collective-permute-start.2 = (bf16[1536,1024]{1,0:T(8,128)(2,1)}, bf16[1536,1024]{1,0:T(8,128)(2,1)}, u32[]{:S(2)}, u32[]{:S(2)}) collective-permute-start(bf16[1536,1024]{1,0:T(8,128)(2,1)} %maximum_select_fusion.3), channel_id=1, source_target_pairs={{0,32},{8,40},{16,48},{24,56},{32,0},{40,8},{48,16},{56,24},{64,96... | collective-permute-start | bytes 9437192 | tf_op jit(solution)/shard_map/ppermute | solution.py:17
  166.0 161.7 %collective-permute-start.3 = (bf16[1536,2048]{1,0:T(8,128)(2,1)}, bf16[1536,2048]{1,0:T(8,128)(2,1)}, u32[]{:S(2)}, u32[]{:S(2)}) collective-permute-start(bf16[1536,2048]{1,0:T(8,128)(2,1)} %maximum_select_fusion.2), channel_id=1, source_target_pairs={{0,64},{8,72},{16,80},{24,88},{32,96},{40,104},{48,112},{56,120},{... | collective-permute-start | bytes 18874376 | tf_op jit(solution)/shard_map/ppermute | solution.py:17
  171.9 151.9 %all-to-all-start.1 = ((bf16[256,16,256]{0,2,1:T(8,128)(2,1)}), bf16[256,16,256]{0,2,1:T(8,128)(2,1)}, u32[]{:S(2)}, u32[]{:S(2)}) async-start(bf16[256,16,256]{0,2,1:T(8,128)(2,1)} %bitcast.8), calls=%async_computation.1 | async-start | bytes 4194304 | tf_op jit(solution)/shard_map/all_to_all | solution.py:62
  176.4 261.4 %all-gather.2.cloned.1.call-start = ((), (), s32[]{:S(2)}) async-start(), calls=%async_computation.4 | async-start | bytes 13369344 | tf_op jit(solution)/shard_map/all_gather | solution.py:71
  485.3 1.2 copy-start.1
  486.5 13.9 %copy-start.4 = (f32[256]{0:T(256)S(1)}, f32[256]{0:T(256)}, u32[]{:S(2)}) copy-start(f32[256]{0:T(256)} %param.15) | copy-start | bytes 3076
  486.5 13.9 %copy-start.5 = (f32[256]{0:T(256)S(1)}, f32[256]{0:T(256)}, u32[]{:S(2)}) copy-start(f32[256]{0:T(256)} %param.14) | copy-start | bytes 3076
Sparse Core Ops, SparseCore 0:
  340.4 97.4 all-gather.1
